TPU v7x, 32 devices: a whole 2x2x4 slice. The times are simulated.
32 devices in a mesh: fs: 8 (over z, y), tp: 4 (over x, core).
Axes of the slice: x: 2, y: 2, z: 4, core: 2. Of those that a mesh axis runs over, the one named last changes fastest.
Arguments:
- h_saved: bfloat16 [4096, 4096], P('fs'), may hold values from -8 to 8
- y_saved: bfloat16 [4096, 2048], P('fs'), may hold values from -8 to 8
- d_gate: bfloat16 [4096, 2048], P('fs', 'tp'), may hold values from -0.25 to 0.25
- d_out: bfloat16 [4096, 4096], P('fs', 'tp'), may hold values from -0.25 to 0.25
- p_gate: bfloat16 [4096, 256], P('fs'), may hold values from -2 to 2
- p_out: bfloat16 [2048, 256], P('fs'), may hold values from -2 to 2
- w_gate: float32 [4096, 2048], P('fs', 'tp'), may hold values from -6 to 6
- w_out: float32 [2048, 4096], P('fs', 'tp'), may hold values from -6 to 6
- m_gate: float32 [256, 2048], P('fs', 'tp'), may hold values from -4 to 4
- m_out: float32 [256, 4096], P('fs', 'tp'), may hold values from -4 to 4
- v_gate: float32 [256, 2048], P('fs', 'tp'), may hold values from 0.02 to 0.2
- v_out: float32 [256, 4096], P('fs', 'tp'), may hold values from 0.02 to 0.2
Outputs:
- step_gate: float32 [4096, 2048], P('fs', 'tp')
- step_out: float32 [2048, 4096], P('fs', 'tp')
- moment_gate: float32 [256, 2048], P('fs', 'tp')
- moment_out: float32 [256, 4096], P('fs', 'tp')
- second_gate: float32 [256, 2048], P('fs', 'tp')
- second_out: float32 [256, 4096], P('fs', 'tp')
- copy_gate: bfloat16 [4096, 2048], P(None, 'tp')
- copy_out: bfloat16 [2048, 4096], P(None, 'tp')
All inputs are finite; a program needn't handle non-finite values.
Results may differ from a plain program's by a relative error of at most 0.001.
Values may be sent and summed in bfloat16 or wider, within the bound.
A program may use at most 64 MiB of HBM per device.

v0:
```python
import jax
import jax.numpy as jnp
from jax import lax
from jax.sharding import PartitionSpec as P

BETA_ONE = 0.9
BETA_TWO = 0.95
LEARN_RATE = 0.1
EPSILON = 1e-06
TOKEN_DIMS = (((0,), (0,)), ((), ()))


def projected_partial(saved, cotangent, factor):
    reduced = jnp.dot(
        saved, lax.all_gather(factor, "fs", axis=0, tiled=True), preferred_element_type=jnp.float32
    )
    return lax.dot_general(
        reduced,
        cotangent.astype(jnp.float32),
        TOKEN_DIMS,
        precision=lax.Precision.HIGHEST,
        preferred_element_type=jnp.float32,
    )


def on_device(
    h_saved, y_saved, d_gate, d_out, p_gate, p_out, w_gate, w_out, m_gate, m_out, v_gate, v_out
):
    part_gate = projected_partial(h_saved, d_gate, p_gate)
    part_out = projected_partial(y_saved, d_out, p_out)
    proj_gate, proj_out = (
        lax.psum_scatter(part_gate, "fs", scatter_dimension=0, tiled=True),
        lax.psum_scatter(part_out, "fs", scatter_dimension=0, tiled=True),
    )
    moment_gate = BETA_ONE * m_gate + (1.0 - BETA_ONE) * proj_gate
    moment_out = BETA_ONE * m_out + (1.0 - BETA_ONE) * proj_out
    second_gate = BETA_TWO * v_gate + (1.0 - BETA_TWO) * proj_gate * proj_gate
    second_out = BETA_TWO * v_out + (1.0 - BETA_TWO) * proj_out * proj_out
    normed_gate = moment_gate / jnp.sqrt(second_gate)
    normed_out = moment_out / jnp.sqrt(second_out)
    whole_gate, whole_out = (
        lax.all_gather(normed_gate, "fs", axis=0, tiled=True),
        lax.all_gather(normed_out, "fs", axis=0, tiled=True),
    )
    update_gate = jnp.dot(p_gate.astype(jnp.float32), whole_gate, precision=lax.Precision.HIGHEST)
    update_out = jnp.dot(p_out.astype(jnp.float32), whole_out, precision=lax.Precision.HIGHEST)
    squares = lax.psum(
        (jnp.sum(update_gate * update_gate), jnp.sum(update_out * update_out)), ("fs", "tp")
    )
    devices_all = lax.axis_size("fs") * lax.axis_size("tp")
    step_gate = update_gate * lax.rsqrt(squares[0] / (update_gate.size * devices_all) + EPSILON)
    step_out = update_out * lax.rsqrt(squares[1] / (update_out.size * devices_all) + EPSILON)
    local_gate = (w_gate - LEARN_RATE * step_gate).astype(jnp.bfloat16)
    local_out = (w_out - LEARN_RATE * step_out).astype(jnp.bfloat16)
    copy_gate, copy_out = (
        lax.all_gather(local_gate, "fs", axis=0, tiled=True),
        lax.all_gather(local_out, "fs", axis=0, tiled=True),
    )
    return (
        step_gate,
        step_out,
        moment_gate,
        moment_out,
        second_gate,
        second_out,
        copy_gate,
        copy_out,
    )


def solution(mesh):
    placed = (
        P("fs", None),
        P("fs", None),
        P("fs", "tp"),
        P("fs", "tp"),
        P("fs", None),
        P("fs", None),
        P("fs", "tp"),
        P("fs", "tp"),
        P("fs", "tp"),
        P("fs", "tp"),
        P("fs", "tp"),
        P("fs", "tp"),
    )
    return jax.shard_map(
        on_device,
        mesh=mesh,
        in_specs=placed,
        out_specs=(
            P("fs", "tp"),
            P("fs", "tp"),
            P("fs", "tp"),
            P("fs", "tp"),
            P("fs", "tp"),
            P("fs", "tp"),
            P(None, "tp"),
            P(None, "tp"),
        ),
        check_vma=False,
    )
```

profile of v0, /device:TPU:0, one launch (start us, length us, event | category | flops | bytes accessed | tf_op | source)
XLA Modules:
  0.0 486.9 jit_solution(17117963242503753305)
XLA Ops:
  7.2 0.0 copy-start
  7.2 0.0 copy-start.1
  7.2 0.0 all-gather.8.cloned.1.call-start
  7.2 0.7 all-gather.8.cloned.1.call-update
  7.9 0.0 all-gather.6.cloned.1.call-start
  8.0 0.7 all-gather.6.cloned.1.call-update
  8.7 0.0 reduce-scatter.5.cloned.1.call-start
  8.7 44.4 %all-gather.8.cloned.1.call-done = bf16[2048,256]{1,0:T(8,128)(2,1)} async-done(((bf16[256,256]{1,0:T(8,128)(2,1)}), bf16[2048,256]{1,0:T(8,128)(2,1)}) %all-gather.8.cloned.1.call-update) | async-done | bytes 1048592 | tf_op jit(solution)/shard_map/all_gather | solution.py:15
  53.2 0.0 copy-done
  53.2 1.9 fusion.6
  55.1 0.0 copy-done.1
  55.1 2.0 fusion.7
  57.1 0.0 reduce-scatter.5.cloned.1.call-update
  57.1 0.0 copy-start.2
  57.2 0.0 reduce-scatter.3.cloned.1.call-start
  57.2 45.9 %all-gather.6.cloned.1.call-done = bf16[4096,256]{1,0:T(8,128)(2,1)} async-done(((bf16[512,256]{1,0:T(8,128)(2,1)}), bf16[4096,256]{1,0:T(8,128)(2,1)}) %all-gather.6.cloned.1.call-update) | async-done | bytes 2097168 | tf_op jit(solution)/shard_map/all_gather | solution.py:15
  103.1 0.0 copy-start.4
  103.1 4.2 fusion.4
  107.3 0.0 copy-done.4
  107.3 0.0 copy-start.3
  107.3 0.0 copy-start.5
  107.3 1.4 fusion.5
  108.7 0.0 reduce-scatter.3.cloned.1.call-update
  108.8 0.0 all-gather.10.cloned.1.call-start
  108.8 61.0 %reduce-scatter.5.cloned.1.call-done = f32[32,1024]{1,0:T(8,128)} async-done(((f32[256,1024]{1,0:T(8,128)}), f32[32,1024]{1,0:T(8,128)}) %reduce-scatter.5.cloned.1.call-update) | async-done | bytes 131088 | tf_op jit(solution)/shard_map/reduce_scatter | solution.py:33
  169.8 1.8 rsqrt_multiply_fusion
  171.6 0.0 all-gather.10.cloned.1.call-update
  171.6 0.0 all-gather.12.cloned.1.call-start
  171.7 0.0 copy-done.2
  171.7 1.3 copy.20
  173.0 62.3 %reduce-scatter.3.cloned.1.call-done = f32[32,512]{1,0:T(8,128)} async-done(((f32[256,512]{1,0:T(8,128)}), f32[32,512]{1,0:T(8,128)}) %reduce-scatter.3.cloned.1.call-update) | async-done | bytes 65552 | tf_op jit(solution)/shard_map/reduce_scatter | solution.py:32
  235.3 1.6 rsqrt_multiply_fusion.1
  236.9 31.7 %all_gather.19 = f32[256,512]{1,0:T(8,128)S(1)} all-gather(f32[32,512]{1,0:T(8,128)S(1)} %get-tuple-element.25), channel_id=1, replica_groups=mesh['fs'=8,'tp'=4] {'fs'}, dimensions={0}, use_global_device_ids=true | all-gather | bytes 589824 | tf_op jit(solution)/shard_map/all_gather | solution.py:42
  268.6 0.0 copy-done.3
  268.6 2.6 multiply_reduce_fusion.1
  271.1 7.3 %all-gather.10.cloned.1.call-done = f32[256,1024]{1,0:T(8,128)} async-done(((f32[32,1024]{1,0:T(8,128)}), f32[256,1024]{1,0:T(8,128)}) %all-gather.10.cloned.1.call-update) | async-done | bytes 1048592 | tf_op jit(solution)/shard_map/all_gather | solution.py:43
  278.4 0.0 copy-done.5
  278.4 2.8 multiply_reduce_fusion
  281.2 38.7 %all-reduce = (f32[]{:T(128)}, f32[]{:T(128)}) all-reduce(f32[]{:T(128)} %get-tuple-element.28, f32[]{:T(128)} %get-tuple-element.30), channel_id=1, replica_groups=mesh['fs'=8,'tp'=4] {'fs','tp'}, use_global_device_ids=true, to_apply=%region_2.0 | all-reduce | flops 2 | bytes 16 | tf_op jit(solution)/shard_map/psum | solution.py:47
  320.6 2.9 subtract_convert_fusion.1
  323.6 0.0 all-gather.12.cloned.1.call-update
  323.6 0.0 all-gather.14.cloned.1.call-start
  323.7 2.5 copy.21
  326.9 2.6 subtract_convert_fusion
  329.4 0.0 all-gather.14.cloned.1.call-update
  329.5 2.5 copy.22
  332.0 2.6 copy.23
  334.6 64.3 %all-gather.12.cloned.1.call-done = bf16[4096,512]{0,1:T(8,128)(2,1)} async-done(((bf16[512,512]{0,1:T(8,128)(2,1)}), bf16[4096,512]{0,1:T(8,128)(2,1)}) %all-gather.12.cloned.1.call-update) | async-done | bytes 4194320 | tf_op jit(solution)/shard_map/all_gather | solution.py:56
  398.8 6.4 %copy.24 = bf16[4096,512]{1,0:T(8,128)(2,1)} copy(bf16[4096,512]{0,1:T(8,128)(2,1)} %all-gather.12.cloned.1.call-done) | data formatting | bytes 8388608
  405.2 68.5 %all-gather.14.cloned.1.call-done = bf16[2048,1024]{0,1:T(8,128)(2,1)} async-done(((bf16[256,1024]{0,1:T(8,128)(2,1)}), bf16[2048,1024]{0,1:T(8,128)(2,1)}) %all-gather.14.cloned.1.call-update) | async-done | bytes 4194320 | tf_op jit(solution)/shard_map/all_gather | solution.py:57
  473.7 6.4 %copy.25 = bf16[2048,1024]{1,0:T(8,128)(2,1)} copy(bf16[2048,1024]{0,1:T(8,128)(2,1)} %all-gather.14.cloned.1.call-done) | data formatting | bytes 8388608
Async XLA Ops:
  7.2 46.0 %copy-start = (bf16[512,2048]{1,0:T(8,128)(2,1)S(1)}, bf16[512,2048]{1,0:T(8,128)(2,1)}, u32[]{:S(2)}) copy-start(bf16[512,2048]{1,0:T(8,128)(2,1)} %param.13) | copy-start | bytes 6291460
  7.2 47.9 %copy-start.1 = (bf16[512,1024]{1,0:T(8,128)(2,1)S(1)}, bf16[512,1024]{1,0:T(8,128)(2,1)}, u32[]{:S(2)}) copy-start(bf16[512,1024]{1,0:T(8,128)(2,1)} %param.15) | copy-start | bytes 3145732
  7.2 46.0 %all-gather.8.cloned.1.call-start = ((), (), s32[]{:S(2)}) async-start(), calls=%async_computation.4 | async-start | bytes 1179648 | tf_op jit(solution)/shard_map/all_gather | solution.py:15
  7.9 95.2 %all-gather.6.cloned.1.call-start = ((), (), s32[]{:S(2)}) async-start(), calls=%async_computation.2 | async-start | bytes 2359296 | tf_op jit(solution)/shard_map/all_gather | solution.py:15
  8.7 161.1 %reduce-scatter.5.cloned.1.call-start = ((), (), s32[]{:S(2)}) async-start(), calls=%async_computation.5 | async-start | bytes 1179648 | tf_op jit(solution)/shard_map/reduce_scatter | solution.py:33
  57.1 114.5 %copy-start.2 = (f32[512,512]{1,0:T(8,128)S(1)}, f32[512,512]{1,0:T(8,128)}, u32[]{:S(2)}) copy-start(f32[512,512]{1,0:T(8,128)} %param.18) | copy-start | bytes 3145732
  57.2 178.1 %reduce-scatter.3.cloned.1.call-start = ((), (), s32[]{:S(2)}) async-start(), calls=%async_computation.3 | async-start | bytes 589824 | tf_op jit(solution)/shard_map/reduce_scatter | solution.py:32
  103.1 4.2 copy-start.4
  107.3 161.3 %copy-start.3 = (bf16[512,256]{1,0:T(8,128)(2,1)S(1)}, bf16[512,256]{1,0:T(8,128)(2,1)}, u32[]{:S(2)}) copy-start(bf16[512,256]{1,0:T(8,128)(2,1)} %param.16) | copy-start | bytes 786436
  107.3 171.1 %copy-start.5 = (bf16[256,256]{1,0:T(8,128)(2,1)S(1)}, bf16[256,256]{1,0:T(8,128)(2,1)}, u32[]{:S(2)}) copy-start(bf16[256,256]{1,0:T(8,128)(2,1)} %param.17) | copy-start | bytes 393220
  108.8 169.6 %all-gather.10.cloned.1.call-start = ((), (), s32[]{:S(2)}) async-start(), calls=%async_computation.6 | async-start | bytes 1179648 | tf_op jit(solution)/shard_map/all_gather | solution.py:43
  171.6 227.2 %all-gather.12.cloned.1.call-start = ((), (), s32[]{:S(2)}) async-start(), calls=%async_computation.7 | async-start | bytes 4718592 | tf_op jit(solution)/shard_map/all_gather | solution.py:56
  323.6 150.1 %all-gather.14.cloned.1.call-start = ((), (), s32[]{:S(2)}) async-start(), calls=%async_computation.8 | async-start | bytes 4718592 | tf_op jit(solution)/shard_map/all_gather | solution.py:57
Sparse Core Ops, SparseCore 0:
  10.1 42.9 all-gather.7
  55.3 47.7 all-gather.5
  107.1 62.6 reduce-scatter.4
  173.6 61.6 reduce-scatter.2
  237.9 40.5 all-gather.9
  323.7 75.0 all-gather.11
  400.9 72.8 all-gather.13
where the time goes:
time: 488 us; the launch traced here: 487 us
  waiting for transfers between devices  355 us (73%)
  blocking collectives  70.4 us (14%)
  local copies, waits for them, and re-layouts  21.8 us (4%)
  between operations  15.6 us (3%)
  matrix products  14.9 us (3%)
  other arithmetic  8.88 us (2%)
    all_gather x2, waiting for transfers between devices, projected_partial(): lax.all_gather(factor, 'fs', axis=0, tiled=True)  90.3 us
    all_gather x1, waiting for transfers between devices, on_device(): lax.all_gather(local_out, 'fs', axis=0, tiled=True)  68.5 us
    all_gather x1, waiting for transfers between devices, on_device(): lax.all_gather(local_gate, 'fs', axis=0, tiled=True)  64.3 us
    reduce_scatter x1, waiting for transfers between devices, on_device(): lax.psum_scatter(part_gate, 'fs', scatter_dimension=0, tiled=True)  62.3 us
    reduce_scatter x1, waiting for transfers between devices, on_device(): lax.psum_scatter(part_out, 'fs', scatter_dimension=0, tiled=True)  61 us
    psum x1, blocking collectives, on_device(): lax.psum((jnp.sum(update_gate * update_gate), jnp.sum(update_out * update...  38.7 us
    all_gather x1, blocking collectives, on_device(): lax.all_gather(normed_gate, 'fs', axis=0, tiled=True)  31.7 us
    unnamed x18, local copies, waits for them, and re-layouts  21.8 us
  transfers between devices with their start and end apart: 7, of which 7 were waited for; matrix products, arithmetic and copies ran while one was open for 7% of the time, Pallas kernels for 0%

commit v1 on v0

--- a/solution.py
+++ b/solution.py
@@ -44,9 +44,9 @@
     )
     update_gate = jnp.dot(p_gate.astype(jnp.float32), whole_gate, precision=lax.Precision.HIGHEST)
     update_out = jnp.dot(p_out.astype(jnp.float32), whole_out, precision=lax.Precision.HIGHEST)
-    squares = lax.psum(
-        (jnp.sum(update_gate * update_gate), jnp.sum(update_out * update_out)), ("fs", "tp")
-    )
+    squares = (jnp.sum(update_gate * update_gate), jnp.sum(update_out * update_out))
+    for axis in ("tp", "fs"):
+        squares = lax.psum(squares, axis)
     devices_all = lax.axis_size("fs") * lax.axis_size("tp")
     step_gate = update_gate * lax.rsqrt(squares[0] / (update_gate.size * devices_all) + EPSILON)
     step_out = update_out * lax.rsqrt(squares[1] / (update_out.size * devices_all) + EPSILON)

time: 488 us -> 472 us (0.967)
  blocking collectives: 70.4 us -> 57.9 us
    psum x1 -> x2, blocking collectives: 38.7 us -> 26.2 us  [on_device(): squares = lax.psum(squares, axis)]
where the time goes in v1:
time: 472 us; the launch traced here: 471 us
  waiting for transfers between devices  352 us (75%)
  blocking collectives  57.9 us (12%)
  local copies, waits for them, and re-layouts  21.8 us (5%)
  between operations  15.6 us (3%)
  matrix products  14.9 us (3%)
  other arithmetic  8.95 us (2%)
    all_gather x2, waiting for transfers between devices, projected_partial(): lax.all_gather(factor, 'fs', axis=0, tiled=True)  90.3 us
    all_gather x1, waiting for transfers between devices, on_device(): lax.all_gather(local_out, 'fs', axis=0, tiled=True)  68.5 us
    reduce_scatter x1, waiting for transfers between devices, on_device(): lax.psum_scatter(part_gate, 'fs', scatter_dimension=0, tiled=True)  62.3 us
    reduce_scatter x1, waiting for transfers between devices, on_device(): lax.psum_scatter(part_out, 'fs', scatter_dimension=0, tiled=True)  61 us
    all_gather x1, waiting for transfers between devices, on_device(): lax.all_gather(local_gate, 'fs', axis=0, tiled=True)  60.8 us
    all_gather x1, blocking collectives, on_device(): lax.all_gather(normed_gate, 'fs', axis=0, tiled=True)  31.7 us
    psum x2, blocking collectives, on_device(): squares = lax.psum(squares, axis)  26.2 us
    unnamed x18, local copies, waits for them, and re-layouts  21.8 us
  transfers between devices with their start and end apart: 7, of which 7 were waited for; matrix products, arithmetic and copies ran while one was open for 7% of the time, Pallas kernels for 0%

profile of v1, /device:TPU:0, one launch (start us, length us, event | category | flops | bytes accessed | tf_op | source)
XLA Modules:
  0.0 471.1 jit_solution(8288790291037191959)
XLA Ops:
  7.2 0.0 copy-start
  7.2 0.0 copy-start.1
  7.2 0.0 all-gather.8.cloned.1.call-start
  7.2 0.7 all-gather.8.cloned.1.call-update
  7.9 0.0 all-gather.6.cloned.1.call-start
  8.0 0.7 all-gather.6.cloned.1.call-update
  8.7 0.0 reduce-scatter.5.cloned.1.call-start
  8.7 44.4 %all-gather.8.cloned.1.call-done = bf16[2048,256]{1,0:T(8,128)(2,1)} async-done(((bf16[256,256]{1,0:T(8,128)(2,1)}), bf16[2048,256]{1,0:T(8,128)(2,1)}) %all-gather.8.cloned.1.call-update) | async-done | bytes 1048592 | tf_op jit(solution)/shard_map/all_gather | solution.py:15
  53.2 0.0 copy-done
  53.2 1.9 fusion.6
  55.1 0.0 copy-done.1
  55.1 2.0 fusion.7
  57.1 0.0 reduce-scatter.5.cloned.1.call-update
  57.1 0.0 copy-start.2
  57.2 0.0 reduce-scatter.3.cloned.1.call-start
  57.2 45.9 %all-gather.6.cloned.1.call-done = bf16[4096,256]{1,0:T(8,128)(2,1)} async-done(((bf16[512,256]{1,0:T(8,128)(2,1)}), bf16[4096,256]{1,0:T(8,128)(2,1)}) %all-gather.6.cloned.1.call-update) | async-done | bytes 2097168 | tf_op jit(solution)/shard_map/all_gather | solution.py:15
  103.1 0.0 copy-start.4
  103.1 4.2 fusion.4
  107.3 0.0 copy-done.4
  107.3 0.0 copy-start.3
  107.3 0.0 copy-start.5
  107.3 1.4 fusion.5
  108.7 0.0 reduce-scatter.3.cloned.1.call-update
  108.8 0.0 all-gather.10.cloned.1.call-start
  108.8 61.0 %reduce-scatter.5.cloned.1.call-done = f32[32,1024]{1,0:T(8,128)} async-done(((f32[256,1024]{1,0:T(8,128)}), f32[32,1024]{1,0:T(8,128)}) %reduce-scatter.5.cloned.1.call-update) | async-done | bytes 131088 | tf_op jit(solution)/shard_map/reduce_scatter | solution.py:33
  169.8 1.8 rsqrt_multiply_fusion
  171.6 0.0 all-gather.10.cloned.1.call-update
  171.6 0.0 all-gather.12.cloned.1.call-start
  171.7 0.0 copy-done.2
  171.7 1.3 copy.20
  173.0 62.3 %reduce-scatter.3.cloned.1.call-done = f32[32,512]{1,0:T(8,128)} async-done(((f32[256,512]{1,0:T(8,128)}), f32[32,512]{1,0:T(8,128)}) %reduce-scatter.3.cloned.1.call-update) | async-done | bytes 65552 | tf_op jit(solution)/shard_map/reduce_scatter | solution.py:32
  235.3 1.6 rsqrt_multiply_fusion.1
  236.9 31.7 %all_gather.19 = f32[256,512]{1,0:T(8,128)S(1)} all-gather(f32[32,512]{1,0:T(8,128)S(1)} %get-tuple-element.27), channel_id=1, replica_groups=mesh['fs'=8,'tp'=4] {'fs'}, dimensions={0}, use_global_device_ids=true | all-gather | bytes 589824 | tf_op jit(solution)/shard_map/all_gather | solution.py:42
  268.6 0.0 copy-done.3
  268.6 2.6 multiply_reduce_fusion.1
  271.1 7.3 %all-gather.10.cloned.1.call-done = f32[256,1024]{1,0:T(8,128)} async-done(((f32[32,1024]{1,0:T(8,128)}), f32[256,1024]{1,0:T(8,128)}) %all-gather.10.cloned.1.call-update) | async-done | bytes 1048592 | tf_op jit(solution)/shard_map/all_gather | solution.py:43
  278.4 0.0 copy-done.5
  278.4 2.8 multiply_reduce_fusion
  281.2 6.3 %all-reduce.1 = (f32[]{:T(128)}, f32[]{:T(128)}) all-reduce(f32[]{:T(128)} %get-tuple-element.30, f32[]{:T(128)} %get-tuple-element.32), channel_id=1, replica_groups=mesh['fs'=8,'tp'=4] {'tp'}, use_global_device_ids=true, to_apply=%region_2.0 | all-reduce | flops 2 | bytes 16 | tf_op jit(solution)/shard_map/psum | solution.py:49
  287.5 19.9 %all-reduce = (f32[]{:T(128)}, f32[]{:T(128)}) all-reduce(f32[]{:T(128)} %get-tuple-element.18, f32[]{:T(128)} %get-tuple-element.19), channel_id=1, replica_groups=mesh['fs'=8,'tp'=4] {'fs'}, use_global_device_ids=true, to_apply=%region_3.0 | all-reduce | flops 2 | bytes 16 | tf_op jit(solution)/shard_map/psum | solution.py:49
  308.1 2.9 subtract_convert_fusion.1
  311.1 0.0 all-gather.12.cloned.1.call-update
  311.1 0.0 all-gather.14.cloned.1.call-start
  311.2 2.5 copy.21
  314.4 2.6 subtract_convert_fusion
  317.0 0.0 all-gather.14.cloned.1.call-update
  317.0 2.6 copy.22
  319.6 2.5 copy.23
  322.1 60.8 %all-gather.12.cloned.1.call-done = bf16[4096,512]{0,1:T(8,128)(2,1)} async-done(((bf16[512,512]{0,1:T(8,128)(2,1)}), bf16[4096,512]{0,1:T(8,128)(2,1)}) %all-gather.12.cloned.1.call-update) | async-done | bytes 4194320 | tf_op jit(solution)/shard_map/all_gather | solution.py:56
  383.0 6.4 %copy.24 = bf16[4096,512]{1,0:T(8,128)(2,1)} copy(bf16[4096,512]{0,1:T(8,128)(2,1)} %all-gather.12.cloned.1.call-done) | data formatting | bytes 8388608
  389.4 68.5 %all-gather.14.cloned.1.call-done = bf16[2048,1024]{0,1:T(8,128)(2,1)} async-done(((bf16[256,1024]{0,1:T(8,128)(2,1)}), bf16[2048,1024]{0,1:T(8,128)(2,1)}) %all-gather.14.cloned.1.call-update) | async-done | bytes 4194320 | tf_op jit(solution)/shard_map/all_gather | solution.py:57
  457.9 6.4 %copy.25 = bf16[2048,1024]{1,0:T(8,128)(2,1)} copy(bf16[2048,1024]{0,1:T(8,128)(2,1)} %all-gather.14.cloned.1.call-done) | data formatting | bytes 8388608
Async XLA Ops:
  7.2 46.0 %copy-start = (bf16[512,2048]{1,0:T(8,128)(2,1)S(1)}, bf16[512,2048]{1,0:T(8,128)(2,1)}, u32[]{:S(2)}) copy-start(bf16[512,2048]{1,0:T(8,128)(2,1)} %param.13) | copy-start | bytes 6291460
  7.2 47.9 %copy-start.1 = (bf16[512,1024]{1,0:T(8,128)(2,1)S(1)}, bf16[512,1024]{1,0:T(8,128)(2,1)}, u32[]{:S(2)}) copy-start(bf16[512,1024]{1,0:T(8,128)(2,1)} %param.15) | copy-start | bytes 3145732
  7.2 46.0 %all-gather.8.cloned.1.call-start = ((), (), s32[]{:S(2)}) async-start(), calls=%async_computation.4 | async-start | bytes 1179648 | tf_op jit(solution)/shard_map/all_gather | solution.py:15
  7.9 95.2 %all-gather.6.cloned.1.call-start = ((), (), s32[]{:S(2)}) async-start(), calls=%async_computation.2 | async-start | bytes 2359296 | tf_op jit(solution)/shard_map/all_gather | solution.py:15
  8.7 161.1 %reduce-scatter.5.cloned.1.call-start = ((), (), s32[]{:S(2)}) async-start(), calls=%async_computation.5 | async-start | bytes 1179648 | tf_op jit(solution)/shard_map/reduce_scatter | solution.py:33
  57.1 114.5 %copy-start.2 = (f32[512,512]{1,0:T(8,128)S(1)}, f32[512,512]{1,0:T(8,128)}, u32[]{:S(2)}) copy-start(f32[512,512]{1,0:T(8,128)} %param.18) | copy-start | bytes 3145732
  57.2 178.1 %reduce-scatter.3.cloned.1.call-start = ((), (), s32[]{:S(2)}) async-start(), calls=%async_computation.3 | async-start | bytes 589824 | tf_op jit(solution)/shard_map/reduce_scatter | solution.py:32
  103.1 4.2 copy-start.4
  107.3 161.3 %copy-start.3 = (bf16[512,256]{1,0:T(8,128)(2,1)S(1)}, bf16[512,256]{1,0:T(8,128)(2,1)}, u32[]{:S(2)}) copy-start(bf16[512,256]{1,0:T(8,128)(2,1)} %param.16) | copy-start | bytes 786436
  107.3 171.1 %copy-start.5 = (bf16[256,256]{1,0:T(8,128)(2,1)S(1)}, bf16[256,256]{1,0:T(8,128)(2,1)}, u32[]{:S(2)}) copy-start(bf16[256,256]{1,0:T(8,128)(2,1)} %param.17) | copy-start | bytes 393220
  108.8 169.6 %all-gather.10.cloned.1.call-start = ((), (), s32[]{:S(2)}) async-start(), calls=%async_computation.6 | async-start | bytes 1179648 | tf_op jit(solution)/shard_map/all_gather | solution.py:43
  171.6 211.4 %all-gather.12.cloned.1.call-start = ((), (), s32[]{:S(2)}) async-start(), calls=%async_computation.7 | async-start | bytes 4718592 | tf_op jit(solution)/shard_map/all_gather | solution.py:56
  311.1 146.8 %all-gather.14.cloned.1.call-start = ((), (), s32[]{:S(2)}) async-start(), calls=%async_computation.8 | async-start | bytes 4718592 | tf_op jit(solution)/shard_map/all_gather | solution.py:57
Sparse Core Ops, SparseCore 0:
  10.1 42.9 all-gather.7
  55.3 47.7 all-gather.5
  107.1 62.6 reduce-scatter.4
  173.6 61.6 reduce-scatter.2
  237.9 40.5 all-gather.9
  311.2 71.6 all-gather.11
  385.0 72.8 all-gather.13
